TPU v7x, 32 devices: a whole 2x2x4 slice. The times are simulated.
32 devices in a mesh: fs: 8 (over z, y), tp: 4 (over x, core).
Axes of the slice: x: 2, y: 2, z: 4, core: 2. Of those that a mesh axis runs over, the one named last changes fastest.
Arguments:
- saved_input: bfloat16 [65536, 2048], P(('fs', 'tp')), may hold values from -500 to 500
- value_cotangent: bfloat16 [65536, 1024], P(('fs', 'tp')), may hold values from -500 to 500
- hidden_input: bfloat16 [65536, 1024], P(('fs', 'tp')), may hold values from -500 to 500
- out_cotangent: bfloat16 [65536, 2048], P(('fs', 'tp')), may hold values from -500 to 500
- value_factor: bfloat16 [2048, 256], P('fs'), may hold values from -2 to 2
- out_factor: bfloat16 [1024, 256], P('fs'), may hold values from -2 to 2
- value_weight: float32 [2048, 1024], P('fs', 'tp'), may hold values from -0.125 to 0.125
- out_weight: float32 [1024, 2048], P('fs', 'tp'), may hold values from -0.1875 to 0.1875
- value_first: float32 [256, 1024], P('fs', 'tp'), may hold values from -1.2 to 1.2
- value_second: float32 [256, 1024], P('fs', 'tp'), may hold values from 0.02 to 0.5
- out_first: float32 [256, 2048], P('fs', 'tp'), may hold values from -1.2 to 1.2
- out_second: float32 [256, 2048], P('fs', 'tp'), may hold values from 0.02 to 0.5
Outputs:
- value_update: float32 [2048, 1024], P('fs', 'tp')
- out_update: float32 [1024, 2048], P('fs', 'tp')
- new_value_weight: float32 [2048, 1024], P('fs', 'tp')
- new_out_weight: float32 [1024, 2048], P('fs', 'tp')
- value_copy: bfloat16 [2048, 1024], P(None, 'tp')
- out_copy: bfloat16 [1024, 2048], P(None, 'tp')
- new_value_first: float32 [256, 1024], P('fs', 'tp')
- new_value_second: float32 [256, 1024], P('fs', 'tp')
- new_out_first: float32 [256, 2048], P('fs', 'tp')
- new_out_second: float32 [256, 2048], P('fs', 'tp')
All inputs are finite; a program needn't handle non-finite values.
Results may differ from a plain program's by a relative error of at most 0.0065.
Values may be sent and summed in bfloat16 or wider, within the bound.
A program may use at most 128 MiB of HBM per device.

v0:
```python
import jax
import jax.numpy as jnp
from jax import lax
from jax.sharding import PartitionSpec as P

D = 2048
DM = 1024
R = 256
momentum_decay = 0.9
square_decay = 0.95
adam_epsilon = 1e-08
update_scale = 0.25
learning_rate = 0.01


def moment_ratio(first, second, lowrank, clip_factor):
    scaled = clip_factor * lowrank
    new_first = momentum_decay * first + (1.0 - momentum_decay) * scaled
    new_second = square_decay * second + (1.0 - square_decay) * scaled * scaled
    ratio = new_first / (jnp.sqrt(new_second) + adam_epsilon)
    return (new_first, new_second, ratio)


def input_times_factor(inputs, factor):
    return jnp.dot(
        inputs, lax.all_gather(factor, "fs", axis=0, tiled=True), preferred_element_type=jnp.float32
    )


def split_product(basis, cotangents):
    basis_high = basis.astype(jnp.bfloat16)
    basis_rest = (basis - basis_high.astype(jnp.float32)).astype(jnp.bfloat16)
    high_part = jnp.einsum("tr,tc->rc", basis_high, cotangents, preferred_element_type=jnp.float32)
    rest_part = jnp.einsum("tr,tc->rc", basis_rest, cotangents, preferred_element_type=jnp.float32)
    return high_part + rest_part


def shards(
    saved_input,
    value_cotangent,
    hidden_input,
    out_cotangent,
    value_factor,
    out_factor,
    value_weight,
    out_weight,
    value_first,
    value_second,
    out_first,
    out_second,
):
    highest = lax.Precision.HIGHEST
    value_basis = input_times_factor(saved_input, value_factor)
    out_basis = input_times_factor(hidden_input, out_factor)
    left = value_basis
    right = out_basis
    first_part = split_product(left, value_cotangent)
    second_part = split_product(right, out_cotangent)
    lowrank = lax.psum_scatter(
        jnp.concatenate([first_part, second_part], axis=1), "fs", scatter_dimension=0, tiled=True
    )
    low_value, low_out = (
        lax.psum_scatter(lowrank[:, :DM], "tp", scatter_dimension=1, tiled=True),
        lax.psum_scatter(lowrank[:, DM:], "tp", scatter_dimension=1, tiled=True),
    )
    squares = lax.psum((jnp.sum(low_value * low_value), jnp.sum(low_out * low_out)), ("fs", "tp"))
    root_mean = jnp.sqrt((squares[0] + squares[1]) / (R * (D + DM)))
    clip_factor = 1.0 / jnp.maximum(root_mean, 1.0)
    new_value_first, new_value_second, value_ratio = moment_ratio(
        value_first, value_second, low_value, clip_factor
    )
    new_out_first, new_out_second, out_ratio = moment_ratio(
        out_first, out_second, low_out, clip_factor
    )
    left = value_factor.astype(jnp.float32)
    right = out_factor.astype(jnp.float32)
    value_sum = jnp.dot(
        left, lax.all_gather(value_ratio, "fs", axis=0, tiled=True), precision=highest
    )
    out_sum = jnp.dot(right, lax.all_gather(out_ratio, "fs", axis=0, tiled=True), precision=highest)
    value_update = update_scale * value_sum
    out_update = update_scale * out_sum
    new_value_weight = value_weight - learning_rate * value_update
    new_out_weight = out_weight - learning_rate * out_update
    value_copy, out_copy = (
        lax.all_gather(new_value_weight.astype(jnp.bfloat16), "fs", axis=0, tiled=True),
        lax.all_gather(new_out_weight.astype(jnp.bfloat16), "fs", axis=0, tiled=True),
    )
    return (
        value_update,
        out_update,
        new_value_weight,
        new_out_weight,
        value_copy,
        out_copy,
        new_value_first,
        new_value_second,
        new_out_first,
        new_out_second,
    )


def solution(mesh):
    placed = (
        P(("fs", "tp"), None),
        P(("fs", "tp"), None),
        P(("fs", "tp"), None),
        P(("fs", "tp"), None),
        P("fs", None),
        P("fs", None),
        P("fs", "tp"),
        P("fs", "tp"),
        P("fs", "tp"),
        P("fs", "tp"),
        P("fs", "tp"),
        P("fs", "tp"),
    )
    return jax.shard_map(
        shards,
        mesh=mesh,
        in_specs=placed,
        out_specs=(
            P("fs", "tp"),
            P("fs", "tp"),
            P("fs", "tp"),
            P("fs", "tp"),
            P(None, "tp"),
            P(None, "tp"),
            P("fs", "tp"),
            P("fs", "tp"),
            P("fs", "tp"),
            P("fs", "tp"),
        ),
        check_vma=False,
    )
```

profile of v0, /device:TPU:0, one launch (start us, length us, event | category | flops | bytes accessed | tf_op | source)
XLA Modules:
  0.0 351.5 jit_solution(5440025133149684813)
XLA Ops:
  7.2 0.0 all-gather.4.cloned.1.call-start
  7.2 0.7 all-gather.4.cloned.1.call-update
  7.9 0.0 reduce-scatter.4.cloned.1.call-start
  8.0 0.0 copy-start
  8.0 33.6 %all_gather.19 = bf16[1024,256]{1,0:T(8,128)(2,1)S(1)} all-gather(bf16[128,256]{1,0:T(8,128)(2,1)} %param.17), channel_id=1, replica_groups=mesh['fs'=8,'tp'=4] {'fs'}, dimensions={0}, use_global_device_ids=true | all-gather | bytes 589824 | tf_op jit(solution)/shard_map/all_gather | solution.py:26
  41.6 3.4 fusion.13
  45.1 0.0 copy-done
  45.1 2.3 fusion.1
  47.4 2.4 convolution_add_fusion
  49.8 4.3 %all-gather.4.cloned.1.call-done = bf16[2048,256]{1,0:T(8,128)(2,1)} async-done(((bf16[256,256]{1,0:T(8,128)(2,1)}), bf16[2048,256]{1,0:T(8,128)(2,1)}) %all-gather.4.cloned.1.call-update) | async-done | bytes 1048592 | tf_op jit(solution)/shard_map/all_gather | solution.py:26
  54.1 0.0 copy-start.10
  54.1 6.2 %fusion.12 = f32[2048,256]{1,0:T(8,128)S(1)} fusion(bf16[2048,2048]{1,0:T(8,128)(2,1)} %param.12, bf16[2048,256]{1,0:T(8,128)(2,1)} %all-gather.4.cloned.1.call-done), kind=kOutput, calls=%fused_computation.27 | convolution fusion | flops 2147483648 | bytes 11534336 | tf_op jit(solution)/shard_map/dot_general | solution.py:25
  60.3 0.0 copy-done.10
  60.3 1.3 fusion.4
  61.6 1.3 convolution_add_fusion.1
  62.9 1.9 pad_maximum_fusion
  64.8 0.0 copy-start.3
  64.8 0.0 copy-start.7
  64.8 0.0 copy-start.4
  64.8 0.0 reduce-scatter.4.cloned.1.call-update
  64.8 0.0 copy-start.8
  64.9 0.0 copy-start.9
  64.9 0.0 copy-start.1
  64.9 0.0 reduce-scatter.6.cloned.1.call-start
  64.9 73.3 %reduce-scatter.4.cloned.1.call-done = f32[32,3072]{1,0:T(8,128)} async-done(((f32[256,3072]{1,0:T(8,128)}), f32[32,3072]{1,0:T(8,128)}) %reduce-scatter.4.cloned.1.call-update) | async-done | bytes 393232 | tf_op jit(solution)/shard_map/reduce_scatter | solution.py:59
  138.3 1.6 slice.8
  139.8 0.0 reduce-scatter.6.cloned.1.call-update
  139.9 0.0 reduce-scatter.8.cloned.1.call-start
  139.9 1.7 slice.9
  141.6 0.0 reduce-scatter.8.cloned.1.call-update
  141.6 0.0 all-gather.8.cloned.1.call-start
  141.7 18.4 %reduce-scatter.6.cloned.1.call-done = f32[32,256]{1,0:T(8,128)} async-done(((f32[32,1024]{1,0:T(8,128)}), f32[32,256]{1,0:T(8,128)}) %reduce-scatter.6.cloned.1.call-update) | async-done | bytes 32784 | tf_op jit(solution)/shard_map/reduce_scatter | solution.py:63
  160.1 1.4 multiply_reduce_fusion.1
  161.5 21.6 %reduce-scatter.8.cloned.1.call-done = f32[32,512]{1,0:T(8,128)} async-done(((f32[32,2048]{1,0:T(8,128)}), f32[32,512]{1,0:T(8,128)}) %reduce-scatter.8.cloned.1.call-update) | async-done | bytes 65552 | tf_op jit(solution)/shard_map/reduce_scatter | solution.py:64
  183.1 1.5 multiply_reduce_fusion
  185.8 0.0 copy-done.3
  185.8 0.1 copy.23
  186.0 39.3 %psum.16 = f32[]{:T(128)} all-reduce(f32[]{:T(128)S(6)} %add.45), channel_id=1, replica_groups=mesh['fs'=8,'tp'=4] {'fs','tp'}, use_global_device_ids=true, to_apply=%region_3.0 | all-reduce | flops 1 | bytes 8 | tf_op jit(solution)/shard_map/psum | solution.py:66
  226.0 0.0 copy-done.6
  226.0 0.0 copy-done.7
  226.0 1.5 add_divide_fusion
  227.6 31.2 %all_gather.21 = f32[256,512]{1,0:T(8,128)S(1)} all-gather(f32[32,512]{1,0:T(8,128)S(1)} %get-tuple-element.24), channel_id=1, replica_groups=mesh['fs'=8,'tp'=4] {'fs'}, dimensions={0}, use_global_device_ids=true | all-gather | bytes 589824 | tf_op jit(solution)/shard_map/all_gather | solution.py:80
  258.8 0.0 copy-done.2
  258.8 1.3 fusion.8
  260.1 0.0 all-gather.8.cloned.1.call-update
  260.1 0.0 all-gather.6.cloned.1.call-start
  260.1 0.0 copy-done.4
  260.1 0.1 copy.22
  260.3 0.0 copy-done.8
  260.3 0.0 copy-done.9
  260.3 0.0 copy-done.5
  260.3 0.6 add_divide_fusion.1
  261.0 31.0 %all_gather.20 = f32[256,256]{1,0:T(8,128)S(1)} all-gather(f32[32,256]{1,0:T(8,128)S(1)} %get-tuple-element.27), channel_id=1, replica_groups=mesh['fs'=8,'tp'=4] {'fs'}, dimensions={0}, use_global_device_ids=true | all-gather | bytes 294912 | tf_op jit(solution)/shard_map/all_gather | solution.py:78
  291.9 0.0 copy-done.1
  291.9 1.0 fusion.9
  293.0 0.0 all-gather.6.cloned.1.call-update
  293.0 0.8 copy.25
  293.9 0.8 copy.27
  294.7 0.8 copy.24
  295.6 0.8 copy.26
  296.4 5.1 %all-gather.8.cloned.1.call-done = bf16[1024,512]{0,1:T(8,128)(2,1)} async-done(((bf16[128,512]{0,1:T(8,128)(2,1)}), bf16[1024,512]{0,1:T(8,128)(2,1)}) %all-gather.8.cloned.1.call-update) | async-done | bytes 1048592 | tf_op jit(solution)/shard_map/all_gather | solution.py:87
  301.5 2.3 copy.29
  303.8 38.6 %all-gather.6.cloned.1.call-done = bf16[2048,256]{0,1:T(8,128)(2,1)} async-done(((bf16[256,256]{0,1:T(8,128)(2,1)}), bf16[2048,256]{0,1:T(8,128)(2,1)}) %all-gather.6.cloned.1.call-update) | async-done | bytes 1048592 | tf_op jit(solution)/shard_map/all_gather | solution.py:86
  342.4 2.3 copy.28
  (5 shorter events, 0.0 us)
Async XLA Ops:
  7.2 46.9 %all-gather.4.cloned.1.call-start = ((), (), s32[]{:S(2)}) async-start(), calls=%async_computation.3 | async-start | bytes 1179648 | tf_op jit(solution)/shard_map/all_gather | solution.py:26
  7.9 130.4 %reduce-scatter.4.cloned.1.call-start = ((), (), s32[]{:S(2)}) async-start(), calls=%async_computation.4 | async-start | bytes 3538944 | tf_op jit(solution)/shard_map/reduce_scatter | solution.py:59
  8.0 37.1 %copy-start = (bf16[2048,2048]{1,0:T(8,128)(2,1)S(1)}, bf16[2048,2048]{1,0:T(8,128)(2,1)}, u32[]{:S(2)}) copy-start(bf16[2048,2048]{1,0:T(8,128)(2,1)} %param.15) | copy-start | bytes 25165828
  54.1 6.3 %copy-start.10 = (bf16[2048,1024]{1,0:T(8,128)(2,1)S(1)}, bf16[2048,1024]{1,0:T(8,128)(2,1)}, u32[]{:S(2)}) copy-start(bf16[2048,1024]{1,0:T(8,128)(2,1)} %param.13) | copy-start | bytes 12582916
  64.8 121.0 %copy-start.3 = (f32[128,512]{1,0:T(8,128)S(1)}, f32[128,512]{1,0:T(8,128)}, u32[]{:S(2)}) copy-start(f32[128,512]{1,0:T(8,128)} %param.19) | copy-start | bytes 786436
  64.8 161.2 %copy-start.6 = (f32[32,512]{1,0:T(8,128)S(1)}, f32[32,512]{1,0:T(8,128)}, u32[]{:S(2)}) copy-start(f32[32,512]{1,0:T(8,128)} %param.23) | copy-start | bytes 196612
  64.8 161.2 %copy-start.7 = (f32[32,512]{1,0:T(8,128)S(1)}, f32[32,512]{1,0:T(8,128)}, u32[]{:S(2)}) copy-start(f32[32,512]{1,0:T(8,128)} %param.22) | copy-start | bytes 196612
  64.8 194.0 %copy-start.2 = (bf16[128,256]{1,0:T(8,128)(2,1)S(1)}, bf16[128,256]{1,0:T(8,128)(2,1)}, u32[]{:S(2)}) copy-start(bf16[128,256]{1,0:T(8,128)(2,1)} %param.17) | copy-start | bytes 196612
  64.8 195.3 %copy-start.4 = (f32[256,256]{1,0:T(8,128)S(1)}, f32[256,256]{1,0:T(8,128)}, u32[]{:S(2)}) copy-start(f32[256,256]{1,0:T(8,128)} %param.18) | copy-start | bytes 786436
  64.8 195.4 %copy-start.8 = (f32[32,256]{1,0:T(8,128)S(1)}, f32[32,256]{1,0:T(8,128)}, u32[]{:S(2)}) copy-start(f32[32,256]{1,0:T(8,128)} %param.21) | copy-start | bytes 98308
  64.9 195.4 %copy-start.9 = (f32[32,256]{1,0:T(8,128)S(1)}, f32[32,256]{1,0:T(8,128)}, u32[]{:S(2)}) copy-start(f32[32,256]{1,0:T(8,128)} %param.20) | copy-start | bytes 98308
  64.9 227.1 %copy-start.1 = (bf16[256,256]{1,0:T(8,128)(2,1)S(1)}, bf16[256,256]{1,0:T(8,128)(2,1)}, u32[]{:S(2)}) copy-start(bf16[256,256]{1,0:T(8,128)(2,1)} %param.16) | copy-start | bytes 393220
  64.9 95.2 %reduce-scatter.6.cloned.1.call-start = ((), (), s32[]{:S(2)}) async-start(), calls=%async_computation.5 | async-start | bytes 163840 | tf_op jit(solution)/shard_map/reduce_scatter | solution.py:63
  139.9 43.2 %reduce-scatter.8.cloned.1.call-start = ((), (), s32[]{:S(2)}) async-start(), calls=%async_computation.6 | async-start | bytes 327680 | tf_op jit(solution)/shard_map/reduce_scatter | solution.py:64
  141.6 159.9 %all-gather.8.cloned.1.call-start = ((), (), s32[]{:S(2)}) async-start(), calls=%async_computation.8 | async-start | bytes 1179648 | tf_op jit(solution)/shard_map/all_gather | solution.py:87
  160.1 100.2 %copy-start.5 = (f32[32,256]{1,0:T(8,128)S(1)}, f32[32,256]{1,0:T(8,128)}, u32[]{:S(2)}) copy-start(f32[32,256]{1,0:T(8,128)} %reduce-scatter.6.cloned.1.call-done) | copy-start | bytes 98308
  260.1 82.4 %all-gather.6.cloned.1.call-start = ((), (), s32[]{:S(2)}) async-start(), calls=%async_computation.7 | async-start | bytes 1179648 | tf_op jit(solution)/shard_map/all_gather | solution.py:86
Sparse Core Ops, SparseCore 0:
  10.1 43.9 all-gather.3
  65.0 73.2 reduce-scatter.3
  141.3 18.7 reduce-scatter.5
  162.9 20.0 reduce-scatter.7
  260.2 41.2 all-gather.7
  304.0 38.3 all-gather.5
where the time goes:
time: 352 us
  waiting for transfers between devices  162 us (46%)
  blocking collectives  135 us (38%)
  matrix products  19.3 us (5%)
  between operations  16.3 us (5%)
  local copies, waits for them, and re-layouts  11.4 us (3%)
  other arithmetic  7.01 us (2%)
    reduce_scatter x1, waiting for transfers between devices, shards(): lax.psum_scatter(jnp.concatenate([first_part, second_part], axis=1), 'fs'...  73.3 us
    psum x1, blocking collectives, shards(): lax.psum((jnp.sum(low_value * low_value), jnp.sum(low_out * low_out)), ('...  39.3 us
    all_gather x1, waiting for transfers between devices, shards(): lax.all_gather(new_value_weight.astype(jnp.bfloat16), 'fs', axis=0, tiled...  38.6 us
    all_gather x1, blocking collectives, input_times_factor(): lax.all_gather(factor, 'fs', axis=0, tiled=True)  33.6 us
    all_gather x1, blocking collectives, shards(): lax.all_gather(out_ratio, 'fs', axis=0, tiled=True)  31.2 us
    all_gather x1, blocking collectives, shards(): lax.all_gather(value_ratio, 'fs', axis=0, tiled=True)  31 us
    reduce_scatter x1, waiting for transfers between devices, shards(): lax.psum_scatter(lowrank[:, DM:], 'tp', scatter_dimension=1, tiled=True)  21.6 us
    reduce_scatter x1, waiting for transfers between devices, shards(): lax.psum_scatter(lowrank[:, :DM], 'tp', scatter_dimension=1, tiled=True)  18.4 us
  transfers between devices with their start and end apart: 6, of which 6 were waited for; matrix products, arithmetic and copies ran while one was open for 5% of the time, Pallas kernels for 0%

commit v1 on v0

--- a/solution.py
+++ b/solution.py
@@ -11,6 +11,27 @@
 adam_epsilon = 1e-08
 update_scale = 0.25
 learning_rate = 0.01
+
+
+def ring_gather(x, axis, dim):
+    size, here, rows = (lax.axis_size(axis), lax.axis_index(axis), x.shape[dim])
+    forward = [(i, (i + 1) % size) for i in range(size)]
+    left = [(i, (i - 1) % size) for i in range(size)]
+    result = jnp.zeros((*x.shape[:dim], size * rows, *x.shape[dim + 1 :]), x.dtype)
+    result = lax.dynamic_update_slice_in_dim(result, x, here * rows, axis=dim)
+    from_left = from_right = x
+    half = size // 2
+    for step in range(1, half + 1):
+        from_left = lax.ppermute(from_left, axis, forward)
+        result = lax.dynamic_update_slice_in_dim(
+            result, from_left, (here - step) % size * rows, axis=dim
+        )
+        if step < size - half:
+            from_right = lax.ppermute(from_right, axis, left)
+            result = lax.dynamic_update_slice_in_dim(
+                result, from_right, (here + step) % size * rows, axis=dim
+            )
+    return result
 
 
 def moment_ratio(first, second, lowrank, clip_factor):
@@ -83,7 +104,7 @@
     new_value_weight = value_weight - learning_rate * value_update
     new_out_weight = out_weight - learning_rate * out_update
     value_copy, out_copy = (
-        lax.all_gather(new_value_weight.astype(jnp.bfloat16), "fs", axis=0, tiled=True),
+        ring_gather(new_value_weight.astype(jnp.bfloat16), "fs", 0),
         lax.all_gather(new_out_weight.astype(jnp.bfloat16), "fs", axis=0, tiled=True),
     )
     return (

time: 352 us -> 335 us (0.952)
  waiting for transfers between devices: 162 us -> 131 us
  starting transfers between devices: 0.24 us -> 15.2 us
    all_gather x1 -> x0, waiting for transfers between devices: 38.6 us -> none  [shards(): lax.all_gather(new_value_weight.astype(jnp.bfloat16), 'fs', axis=0, tiled...]
    ppermute x0 -> x7, starting transfers between devices: none -> 15 us  [the longest x3 9.35 us: ring_gather(): from_right = lax.ppermute(from_right, axis, left)]
    ppermute x0 -> x7, waiting for transfers between devices: none -> 12.6 us  [the longest x4 8.4 us: ring_gather(): from_left = lax.ppermute(from_left, axis, forward)]
    all_gather x1, waiting for transfers between devices: 5.13 us -> 0.02 us  [shards(): lax.all_gather(new_out_weight.astype(jnp.bfloat16), 'fs', axis=0, tiled=T...]
    unnamed x30 -> x29, local copies, waits for them, and re-layouts: 8.18 us -> 6.28 us
  transfers between devices with their start and end apart: 6 -> 12, of which waited for: 6 -> 10; matrix products, arithmetic and copies ran while one was open for 5% -> 5% of each run, Pallas kernels for 0% -> 0%
where the time goes in v1:
time: 335 us
  blocking collectives  135 us (40%)
  waiting for transfers between devices  131 us (39%)
  matrix products  18.6 us (6%)
  between operations  16.3 us (5%)
  starting transfers between devices  15.2 us (5%)
  local copies, waits for them, and re-layouts  10.5 us (3%)
  other arithmetic  7.69 us (2%)
    reduce_scatter x1, waiting for transfers between devices, shards(): lax.psum_scatter(jnp.concatenate([first_part, second_part], axis=1), 'fs'...  73.5 us
    psum x1, blocking collectives, shards(): lax.psum((jnp.sum(low_value * low_value), jnp.sum(low_out * low_out)), ('...  39.3 us
    all_gather x1, blocking collectives, input_times_factor(): lax.all_gather(factor, 'fs', axis=0, tiled=True)  33.6 us
    all_gather x1, blocking collectives, shards(): lax.all_gather(value_ratio, 'fs', axis=0, tiled=True)  31.3 us
    all_gather x1, blocking collectives, shards(): lax.all_gather(out_ratio, 'fs', axis=0, tiled=True)  31.3 us
    reduce_scatter x1, waiting for transfers between devices, shards(): lax.psum_scatter(lowrank[:, DM:], 'tp', scatter_dimension=1, tiled=True)  21.6 us
    reduce_scatter x1, waiting for transfers between devices, shards(): lax.psum_scatter(lowrank[:, :DM], 'tp', scatter_dimension=1, tiled=True)  17.9 us
    dot_general x2, matrix products, input_times_factor(): jnp.dot(inputs, lax.all_gather(factor, 'fs', axis=0, tiled=True), preferr...  9.69 us
  transfers between devices with their start and end apart: 12, of which 10 were waited for; matrix products, arithmetic and copies ran while one was open for 5% of the time, Pallas kernels for 0%

profile of v1, /device:TPU:0, one launch (start us, length us, event | category | flops | bytes accessed | tf_op | source)
XLA Modules:
  0.0 334.5 jit_solution(476626272279408948)
XLA Ops:
  7.2 0.0 all-gather.3.cloned.1.call-start
  7.2 0.7 all-gather.3.cloned.1.call-update
  7.9 0.0 reduce-scatter.4.cloned.1.call-start
  8.0 33.6 %all_gather.16 = bf16[1024,256]{1,0:T(8,128)(2,1)S(1)} all-gather(bf16[128,256]{1,0:T(8,128)(2,1)} %param.17), channel_id=1, replica_groups=mesh['fs'=8,'tp'=4] {'fs'}, dimensions={0}, use_global_device_ids=true | all-gather | bytes 589824 | tf_op jit(solution)/shard_map/all_gather | solution.py:47
  41.6 3.4 %fusion.13 = f32[2048,256]{1,0:T(8,128)S(1)} fusion(bf16[2048,1024]{1,0:T(8,128)(2,1)} %param.14, bf16[1024,256]{1,0:T(8,128)(2,1)S(1)} %all_gather.16), kind=kOutput, calls=%fused_computation.36 | convolution fusion | flops 1073741824 | bytes 6815744 | tf_op jit(solution)/shard_map/dot_general | solution.py:46
  45.1 2.3 fusion.1
  47.4 2.4 convolution_add_fusion
  49.8 4.3 %all-gather.3.cloned.1.call-done = bf16[2048,256]{1,0:T(8,128)(2,1)} async-done(((bf16[256,256]{1,0:T(8,128)(2,1)}), bf16[2048,256]{1,0:T(8,128)(2,1)}) %all-gather.3.cloned.1.call-update) | async-done | bytes 1048592 | tf_op jit(solution)/shard_map/all_gather | solution.py:47
  54.1 6.2 %fusion.12 = f32[2048,256]{1,0:T(8,128)S(1)} fusion(bf16[2048,2048]{1,0:T(8,128)(2,1)} %param.12, bf16[2048,256]{1,0:T(8,128)(2,1)} %all-gather.3.cloned.1.call-done), kind=kOutput, calls=%fused_computation.35 | convolution fusion | flops 2147483648 | bytes 11534336 | tf_op jit(solution)/shard_map/dot_general | solution.py:46
  60.3 1.3 fusion.4
  61.6 1.3 convolution_add_fusion.1
  62.9 1.9 pad_maximum_fusion
  64.8 0.0 reduce-scatter.4.cloned.1.call-update
  64.9 0.0 reduce-scatter.6.cloned.1.call-start
  64.9 73.5 %reduce-scatter.4.cloned.1.call-done = f32[32,3072]{1,0:T(8,128)} async-done(((f32[256,3072]{1,0:T(8,128)}), f32[32,3072]{1,0:T(8,128)}) %reduce-scatter.4.cloned.1.call-update) | async-done | bytes 393232 | tf_op jit(solution)/shard_map/reduce_scatter | solution.py:80
  138.4 1.6 slice.8
  140.0 0.0 reduce-scatter.6.cloned.1.call-update
  140.0 0.0 reduce-scatter.8.cloned.1.call-start
  140.1 1.7 slice.9
  141.8 0.0 reduce-scatter.8.cloned.1.call-update
  141.8 0.0 all-gather.5.cloned.1.call-start
  142.0 0.1 copy.22
  142.1 0.1 copy.23
  142.3 17.9 %reduce-scatter.6.cloned.1.call-done = f32[32,256]{1,0:T(8,128)} async-done(((f32[32,1024]{1,0:T(8,128)}), f32[32,256]{1,0:T(8,128)}) %reduce-scatter.6.cloned.1.call-update) | async-done | bytes 32784 | tf_op jit(solution)/shard_map/reduce_scatter | solution.py:84
  160.2 1.4 multiply_reduce_fusion.1
  161.6 21.6 %reduce-scatter.8.cloned.1.call-done = f32[32,512]{1,0:T(8,128)} async-done(((f32[32,2048]{1,0:T(8,128)}), f32[32,512]{1,0:T(8,128)}) %reduce-scatter.8.cloned.1.call-update) | async-done | bytes 65552 | tf_op jit(solution)/shard_map/reduce_scatter | solution.py:85
  183.2 1.5 multiply_reduce_fusion
  185.9 39.3 %psum.16 = f32[]{:T(128)} all-reduce(f32[]{:T(128)S(6)} %add.104), channel_id=1, replica_groups=mesh['fs'=8,'tp'=4] {'fs','tp'}, use_global_device_ids=true, to_apply=%region_3.0 | all-reduce | flops 1 | bytes 8 | tf_op jit(solution)/shard_map/psum | solution.py:87
  226.0 1.5 add_divide_fusion
  227.5 31.3 %all_gather.18 = f32[256,512]{1,0:T(8,128)S(1)} all-gather(f32[32,512]{1,0:T(8,128)S(1)} %get-tuple-element.24), channel_id=1, replica_groups=mesh['fs'=8,'tp'=4] {'fs'}, dimensions={0}, use_global_device_ids=true | all-gather | bytes 589824 | tf_op jit(solution)/shard_map/all_gather | solution.py:101
  258.8 1.3 fusion.8
  260.1 0.0 all-gather.5.cloned.1.call-update
  260.1 1.4 add_divide_fusion.1
  261.5 31.3 %all_gather.17 = f32[256,256]{1,0:T(8,128)S(1)} all-gather(f32[32,256]{1,0:T(8,128)S(1)} %get-tuple-element.27), channel_id=1, replica_groups=mesh['fs'=8,'tp'=4] {'fs'}, dimensions={0}, use_global_device_ids=true | all-gather | bytes 294912 | tf_op jit(solution)/shard_map/all_gather | solution.py:99
  292.8 0.4 fusion.9
  293.2 2.7 collective-permute-start
  295.9 2.1 collective-permute-start.1
  298.0 0.1 copy.24
  298.1 0.1 broadcast_in_dim.3
  298.2 0.8 copy.33
  299.1 0.8 copy.35
  299.9 0.8 copy.32
  300.7 0.8 copy.34
  301.6 0.1 copy.25
  301.7 2.5 collective-permute-start.2
  304.2 0.8 collective-permute-done.1
  305.0 0.1 copy.26
  305.1 3.3 collective-permute-start.3
  308.4 1.1 collective-permute-done.2
  309.5 0.1 copy.27
  309.6 0.4 collective-permute-start.4
  310.0 2.2 collective-permute-done.3
  312.2 0.1 copy.28
  312.3 4.0 %collective-permute-start.5 = (bf16[256,256]{0,1:T(8,128)(2,1)S(1)}, bf16[256,256]{0,1:T(8,128)(2,1)S(1)}, u32[]{:S(2)}, u32[]{:S(2)}) collective-permute-start(bf16[256,256]{0,1:T(8,128)(2,1)S(1)} %collective-permute-done.3), channel_id=1, source_target_pairs={{0,28},{4,0},{8,4},{12,8},{16,12},{20,16},{24,20},{28,24},{1,29},{... | collective-permute-start | bytes 393224 | tf_op jit(solution)/shard_map/ppermute | solution.py:30
  316.3 1.1 collective-permute-done.4
  317.4 0.1 copy.29
  317.5 0.1 collective-permute-start.6
  317.6 1.2 collective-permute-done.5
  318.8 0.1 copy.30
  318.9 6.3 %collective-permute-done.6 = bf16[256,256]{0,1:T(8,128)(2,1)S(1)} collective-permute-done((bf16[256,256]{0,1:T(8,128)(2,1)S(1)}, bf16[256,256]{0,1:T(8,128)(2,1)S(1)}, u32[]{:S(2)}, u32[]{:S(2)}) %collective-permute-start.6) | collective-permute-done | bytes 131104 | tf_op jit(solution)/shard_map/ppermute | solution.py:25
  325.2 0.1 copy.31
  325.3 0.0 copy-start.1
  325.4 0.0 all-gather.5.cloned.1.call-done
  325.4 2.6 copy.36
  (32 shorter events, 0.2 us)
Async XLA Ops:
  7.2 46.9 %all-gather.3.cloned.1.call-start = ((), (), s32[]{:S(2)}) async-start(), calls=%async_computation.3 | async-start | bytes 1179648 | tf_op jit(solution)/shard_map/all_gather | solution.py:47
  7.9 130.5 %reduce-scatter.4.cloned.1.call-start = ((), (), s32[]{:S(2)}) async-start(), calls=%async_computation.4 | async-start | bytes 3538944 | tf_op jit(solution)/shard_map/reduce_scatter | solution.py:80
  8.0 37.1 %copy-start = (bf16[2048,2048]{1,0:T(8,128)(2,1)S(1)}, bf16[2048,2048]{1,0:T(8,128)(2,1)}, u32[]{:S(2)}) copy-start(bf16[2048,2048]{1,0:T(8,128)(2,1)} %param.15) | copy-start | bytes 25165828
  54.1 6.2 %copy-start.10 = (bf16[2048,1024]{1,0:T(8,128)(2,1)S(1)}, bf16[2048,1024]{1,0:T(8,128)(2,1)}, u32[]{:S(2)}) copy-start(bf16[2048,1024]{1,0:T(8,128)(2,1)} %param.13) | copy-start | bytes 12582916
  64.8 77.2 %copy-start.4 = (f32[256,256]{1,0:T(8,128)S(1)}, f32[256,256]{1,0:T(8,128)}, u32[]{:S(2)}) copy-start(f32[256,256]{1,0:T(8,128)} %param.18) | copy-start | bytes 786436
  64.8 77.3 %copy-start.5 = (f32[128,512]{1,0:T(8,128)S(1)}, f32[128,512]{1,0:T(8,128)}, u32[]{:S(2)}) copy-start(f32[128,512]{1,0:T(8,128)} %param.19) | copy-start | bytes 786436
  64.8 161.2 %copy-start.6 = (f32[32,512]{1,0:T(8,128)S(1)}, f32[32,512]{1,0:T(8,128)}, u32[]{:S(2)}) copy-start(f32[32,512]{1,0:T(8,128)} %param.23) | copy-start | bytes 196612
  64.8 161.2 %copy-start.7 = (f32[32,512]{1,0:T(8,128)S(1)}, f32[32,512]{1,0:T(8,128)}, u32[]{:S(2)}) copy-start(f32[32,512]{1,0:T(8,128)} %param.22) | copy-start | bytes 196612
  64.8 194.0 %copy-start.3 = (bf16[128,256]{1,0:T(8,128)(2,1)S(1)}, bf16[128,256]{1,0:T(8,128)(2,1)}, u32[]{:S(2)}) copy-start(bf16[128,256]{1,0:T(8,128)(2,1)} %param.17) | copy-start | bytes 196612
  64.8 195.2 %copy-start.8 = (f32[32,256]{1,0:T(8,128)S(1)}, f32[32,256]{1,0:T(8,128)}, u32[]{:S(2)}) copy-start(f32[32,256]{1,0:T(8,128)} %param.21) | copy-start | bytes 98308
  64.9 195.2 %copy-start.9 = (f32[32,256]{1,0:T(8,128)S(1)}, f32[32,256]{1,0:T(8,128)}, u32[]{:S(2)}) copy-start(f32[32,256]{1,0:T(8,128)} %param.20) | copy-start | bytes 98308
  64.9 227.9 %copy-start.2 = (bf16[256,256]{1,0:T(8,128)(2,1)S(1)}, bf16[256,256]{1,0:T(8,128)(2,1)}, u32[]{:S(2)}) copy-start(bf16[256,256]{1,0:T(8,128)(2,1)} %param.16) | copy-start | bytes 393220
  64.9 95.3 %reduce-scatter.6.cloned.1.call-start = ((), (), s32[]{:S(2)}) async-start(), calls=%async_computation.5 | async-start | bytes 163840 | tf_op jit(solution)/shard_map/reduce_scatter | solution.py:84
  140.0 43.1 %reduce-scatter.8.cloned.1.call-start = ((), (), s32[]{:S(2)}) async-start(), calls=%async_computation.6 | async-start | bytes 327680 | tf_op jit(solution)/shard_map/reduce_scatter | solution.py:85
  141.8 183.6 %all-gather.5.cloned.1.call-start = ((), (), s32[]{:S(2)}) async-start(), calls=%async_computation.7 | async-start | bytes 1179648 | tf_op jit(solution)/shard_map/all_gather | solution.py:108
  293.2 8.4 %collective-permute-start = (bf16[256,256]{0,1:T(8,128)(2,1)S(1)}, bf16[256,256]{0,1:T(8,128)(2,1)S(1)}, u32[]{:S(2)}, u32[]{:S(2)}) collective-permute-start(bf16[256,256]{0,1:T(8,128)(2,1)S(1)} %get-tuple-element.22), channel_id=1, source_target_pairs={{0,4},{4,8},{8,12},{12,16},{16,20},{20,24},{24,28},{28,0},{1,5},{5... | collective-permute-start | bytes 393224 | tf_op jit(solution)/shard_map/ppermute | solution.py:25
  295.9 9.1 %collective-permute-start.1 = (bf16[256,256]{0,1:T(8,128)(2,1)S(1)}, bf16[256,256]{0,1:T(8,128)(2,1)S(1)}, u32[]{:S(2)}, u32[]{:S(2)}) collective-permute-start(bf16[256,256]{0,1:T(8,128)(2,1)S(1)} %get-tuple-element.22), channel_id=1, source_target_pairs={{0,28},{4,0},{8,4},{12,8},{16,12},{20,16},{24,20},{28,24},{1,29},{... | collective-permute-start | bytes 393224 | tf_op jit(solution)/shard_map/ppermute | solution.py:30
  301.7 7.8 %collective-permute-start.2 = (bf16[256,256]{0,1:T(8,128)(2,1)S(1)}, bf16[256,256]{0,1:T(8,128)(2,1)S(1)}, u32[]{:S(2)}, u32[]{:S(2)}) collective-permute-start(bf16[256,256]{0,1:T(8,128)(2,1)S(1)} %collective-permute-done), channel_id=1, source_target_pairs={{0,4},{4,8},{8,12},{12,16},{16,20},{20,24},{24,28},{28,0},{1,5},{5... | collective-permute-start | bytes 393224 | tf_op jit(solution)/shard_map/ppermute | solution.py:25
  305.1 7.1 %collective-permute-start.3 = (bf16[256,256]{0,1:T(8,128)(2,1)S(1)}, bf16[256,256]{0,1:T(8,128)(2,1)S(1)}, u32[]{:S(2)}, u32[]{:S(2)}) collective-permute-start(bf16[256,256]{0,1:T(8,128)(2,1)S(1)} %collective-permute-done.1), channel_id=1, source_target_pairs={{0,28},{4,0},{8,4},{12,8},{16,12},{20,16},{24,20},{28,24},{1,29},{... | collective-permute-start | bytes 393224 | tf_op jit(solution)/shard_map/ppermute | solution.py:30
  309.6 7.8 %collective-permute-start.4 = (bf16[256,256]{0,1:T(8,128)(2,1)S(1)}, bf16[256,256]{0,1:T(8,128)(2,1)S(1)}, u32[]{:S(2)}, u32[]{:S(2)}) collective-permute-start(bf16[256,256]{0,1:T(8,128)(2,1)S(1)} %collective-permute-done.2), channel_id=1, source_target_pairs={{0,4},{4,8},{8,12},{12,16},{16,20},{20,24},{24,28},{28,0},{1,5},{5... | collective-permute-start | bytes 393224 | tf_op jit(solution)/shard_map/ppermute | solution.py:25
  312.3 6.5 %collective-permute-start.5 = (bf16[256,256]{0,1:T(8,128)(2,1)S(1)}, bf16[256,256]{0,1:T(8,128)(2,1)S(1)}, u32[]{:S(2)}, u32[]{:S(2)}) collective-permute-start(bf16[256,256]{0,1:T(8,128)(2,1)S(1)} %collective-permute-done.3), channel_id=1, source_target_pairs={{0,28},{4,0},{8,4},{12,8},{16,12},{20,16},{24,20},{28,24},{1,29},{... | collective-permute-start | bytes 393224 | tf_op jit(solution)/shard_map/ppermute | solution.py:30
  317.5 7.7 %collective-permute-start.6 = (bf16[256,256]{0,1:T(8,128)(2,1)S(1)}, bf16[256,256]{0,1:T(8,128)(2,1)S(1)}, u32[]{:S(2)}, u32[]{:S(2)}) collective-permute-start(bf16[256,256]{0,1:T(8,128)(2,1)S(1)} %collective-permute-done.4), channel_id=1, source_target_pairs={{0,4},{4,8},{8,12},{12,16},{16,20},{20,24},{24,28},{28,0},{1,5},{5... | collective-permute-start | bytes 393224 | tf_op jit(solution)/shard_map/ppermute | solution.py:25
  325.3 2.7 copy-start.1
Sparse Core Ops, SparseCore 0:
  10.1 43.9 all-gather.2
  65.0 73.4 reduce-scatter.3
  141.4 18.7 reduce-scatter.5
  163.1 20.0 reduce-scatter.7
  260.2 44.4 all-gather.4
